TPU v7x, 32 devices: a whole 2x2x4 slice. The times are simulated.
32 devices in a mesh: sp: 8 (over z, x), tp: 4 (over y, core).
Axes of the slice: x: 2, y: 2, z: 4, core: 2. Of those that a mesh axis runs over, the one named last changes fastest.
Arguments:
- cotangent: bfloat16 [1024, 2048], P('sp'), may hold values from -6 to 6
- layer_input: bfloat16 [1024, 2048], P('sp'), may hold values from -6 to 6
- group_choice: int32 [1024], P('sp'), may hold values from 0 to 1, as said below
- inner_pair: int32 [1024, 2], P('sp'), may hold values from 0 to 3, as said below
- group_weight: float32 [1024], P('sp'), may hold values from 0.25 to 1
- inner_logits: float32 [1024, 2], P('sp'), may hold values from -6 to 6
- w_gate: bfloat16 [8, 2048, 2048], P('sp', 'tp'), may hold values from -0.125 to 0.125
- w_up: bfloat16 [8, 2048, 2048], P('sp', 'tp'), may hold values from -0.125 to 0.125
- w_down: bfloat16 [8, 2048, 2048], P('sp', 'tp'), may hold values from -0.125 to 0.125
- outer_gate: bfloat16 [2048, 1024], P('tp', 'sp'), may hold values from -6 to 6
- inner_gate: bfloat16 [2048, 1024], P('tp', 'sp'), may hold values from -6 to 6
- value_stream: bfloat16 [2048, 1024], P('tp', 'sp'), may hold values from -6 to 6
- conv_out: bfloat16 [2048, 1024], P('tp', 'sp'), may hold values from -6 to 6
- conv_taps: float32 [3, 2048], P(None, 'tp'), may hold values from -4 to 4
- w_out: bfloat16 [2048, 2048], P(None, 'tp'), may hold values from -0.125 to 0.125
Outputs:
- grad_input: bfloat16 [1024, 2048], P('sp', 'tp')
- grad_w_gate: bfloat16 [8, 2048, 2048], P('sp', 'tp')
- grad_w_up: bfloat16 [8, 2048, 2048], P('sp', 'tp')
- grad_w_down: bfloat16 [8, 2048, 2048], P('sp', 'tp')
- grad_w_out: float32 [2048, 2048], P('sp', 'tp')
- grad_outer_gate: bfloat16 [2048, 1024], P('tp', 'sp')
- grad_inner_gate: bfloat16 [2048, 1024], P('tp', 'sp')
- grad_value_stream: bfloat16 [2048, 1024], P('tp', 'sp')
Inputs may be any that keep to these rules, and one draw needn't show every extreme that they name: Within each block of 128 positions of the sp order, every expert 4 * group_choice + inner_pair is named by at most 52 positions; in every block the 4 experts of one group, the same group for all blocks, are each named by exactly 52 positions. `inner_pair`: the two entries of a position differ.
All inputs are finite; a program needn't handle non-finite values.
Results may differ from a plain program's by a relative error of at most 0.019.
Values may be sent and summed in bfloat16 or wider, within the bound.
A program may use at most 64 MiB of HBM per device.

v0:
```python
import jax
import jax.numpy as jnp
from jax import lax
from jax.sharding import PartitionSpec as P

TAPS = 3
INNER = 4


def from_behind(value, axis, steps):
    count = lax.axis_size(axis)
    first, last = (max(0, -steps), min(count, count - steps))
    return lax.ppermute(value, axis, [(source, source + steps) for source in range(first, last)])


def pack_rows(input_rows, cot_rows, token_of, entry_of, filled, routing_flat, experts, capacity):
    picked = jnp.where(filled[:, None], input_rows[token_of], jnp.zeros((), jnp.bfloat16))
    weighted = routing_flat[entry_of][:, None] * cot_rows[token_of].astype(jnp.float32)
    scaled = jnp.where(filled[:, None], weighted, 0.0).astype(jnp.bfloat16)
    return (picked.reshape(experts, capacity, -1), scaled.reshape(experts, capacity, -1))


def per_device(
    cotangent,
    layer_input,
    group_choice,
    inner_pair,
    group_weight,
    inner_logits,
    w_gate,
    w_up,
    w_down,
    outer_gate,
    inner_gate,
    value_stream,
    conv_out,
    conv_taps,
    w_out,
):
    experts = lax.axis_size("sp")
    tok_rows = cotangent.shape[0]
    model_width = cotangent.shape[1]
    col_piece = model_width // lax.axis_size("tp")
    column = lax.axis_index("tp") * col_piece
    group_count = experts // INNER
    capacity = 4 * (3 * tok_rows // (16 * group_count) + 1)
    entry_count = 2 * tok_rows
    expert_ids = (INNER * group_choice[:, None] + inner_pair).reshape(-1)
    onehot = (expert_ids[:, None] == jnp.arange(experts, dtype=jnp.int32)[None, :]).astype(
        jnp.int32
    )
    position = jnp.sum((jnp.cumsum(onehot, axis=0) - onehot) * onehot, axis=1)
    target = expert_ids * capacity + position
    source = (
        jnp.full((experts * capacity,), entry_count, jnp.int32)
        .at[target]
        .set(jnp.arange(entry_count, dtype=jnp.int32))
    )
    filled = source < entry_count
    entry_of = jnp.minimum(source, entry_count - 1)
    token_of = entry_of // 2
    routing = group_weight[:, None] * jax.nn.softmax(inner_logits, axis=1)
    routing_flat = routing.reshape(-1)
    input_cols = lax.dynamic_slice_in_dim(layer_input, column, col_piece, 1)
    cot_cols = lax.dynamic_slice_in_dim(cotangent, column, col_piece, 1)
    input_send, scaled_send = pack_rows(
        input_cols, cot_cols, token_of, entry_of, filled, routing_flat, experts, capacity
    )
    input_part, scaled_part = (
        lax.all_to_all(input_send, "sp", split_axis=0, concat_axis=0, tiled=True),
        lax.all_to_all(scaled_send, "sp", split_axis=0, concat_axis=0, tiled=True),
    )
    input_recv, scaled_recv = (
        lax.all_gather(input_part, "tp", axis=2, tiled=True),
        lax.all_gather(scaled_part, "tp", axis=2, tiled=True),
    )
    in_rows = input_recv.reshape(-1, model_width)
    scaled_rows = scaled_recv.reshape(-1, model_width)
    gate_weight = w_gate[0]
    up_weight = w_up[0]
    down_weight = w_down[0]
    inner_dims = (((1,), (1,)), ((), ()))
    row_dims = (((0,), (0,)), ((), ()))
    gate_pre = lax.dot_general(in_rows, gate_weight, inner_dims, preferred_element_type=jnp.float32)
    up_pre = lax.dot_general(in_rows, up_weight, inner_dims, preferred_element_type=jnp.float32)
    back = lax.dot_general(scaled_rows, down_weight, inner_dims, preferred_element_type=jnp.float32)
    sigmoid_gate = jax.nn.sigmoid(gate_pre)
    silu_gate = gate_pre * sigmoid_gate
    hidden = (silu_gate * up_pre).astype(jnp.bfloat16)
    grad_gate = (back * up_pre * sigmoid_gate * (1.0 + gate_pre * (1.0 - sigmoid_gate))).astype(
        jnp.bfloat16
    )
    grad_up = (back * silu_gate).astype(jnp.bfloat16)
    partial_rows = jnp.dot(grad_gate, gate_weight, preferred_element_type=jnp.float32) + jnp.dot(
        grad_up, up_weight, preferred_element_type=jnp.float32
    )
    grad_w_gate = lax.dot_general(
        grad_gate, in_rows, row_dims, preferred_element_type=jnp.float32
    ).astype(jnp.bfloat16)
    grad_w_up = lax.dot_general(
        grad_up, in_rows, row_dims, preferred_element_type=jnp.float32
    ).astype(jnp.bfloat16)
    grad_w_down = lax.dot_general(
        hidden, scaled_rows, row_dims, preferred_element_type=jnp.float32
    ).astype(jnp.bfloat16)
    shares = lax.psum_scatter(
        partial_rows.astype(jnp.bfloat16), "tp", scatter_dimension=1, tiled=True
    )
    returned = lax.all_to_all(
        shares.reshape(experts, capacity, col_piece), "sp", split_axis=0, concat_axis=0, tiled=True
    )
    back_tok = (
        returned.reshape(-1, col_piece)[target].reshape(tok_rows, 2, col_piece).astype(jnp.float32)
    )
    cot_cols = lax.dynamic_slice_in_dim(cotangent, column, col_piece, 1).astype(jnp.float32)
    own_cols = (cot_cols + back_tok[:, 0] + back_tok[:, 1]).astype(jnp.bfloat16)
    grad_rows = lax.all_gather(own_cols, "tp", axis=1, tiled=True)
    grad_out = lax.dot_general(
        w_out, grad_rows, (((0,), (1,)), ((), ())), preferred_element_type=jnp.float32
    )
    mixer_out = (outer_gate.astype(jnp.float32) * conv_out.astype(jnp.float32)).astype(jnp.bfloat16)
    grad_w_out = lax.psum_scatter(
        lax.dot_general(
            grad_rows, mixer_out, (((0,), (1,)), ((), ())), preferred_element_type=jnp.float32
        ).astype(jnp.bfloat16),
        "sp",
        scatter_dimension=0,
        tiled=True,
    ).astype(jnp.float32)
    grad_outer_gate = (grad_out * conv_out.astype(jnp.float32)).astype(jnp.bfloat16)
    grad_conv = grad_out * outer_gate.astype(jnp.float32)
    following = from_behind(grad_conv[:, : TAPS - 1], "sp", -1)
    extended = jnp.concatenate([grad_conv, following], axis=1)
    grad_mixed = jnp.zeros_like(grad_conv)
    for offset in range(TAPS):
        start = TAPS - 1 - offset
        grad_mixed = grad_mixed + conv_taps[offset][:, None] * extended[:, start : start + tok_rows]
    grad_inner_gate = (grad_mixed * value_stream.astype(jnp.float32)).astype(jnp.bfloat16)
    grad_value_stream = (grad_mixed * inner_gate.astype(jnp.float32)).astype(jnp.bfloat16)
    return (
        own_cols,
        grad_w_gate[None],
        grad_w_up[None],
        grad_w_down[None],
        grad_w_out,
        grad_outer_gate,
        grad_inner_gate,
        grad_value_stream,
    )


def solution(mesh):
    return jax.shard_map(
        per_device,
        mesh=mesh,
        in_specs=(
            P("sp", None),
            P("sp", None),
            P("sp"),
            P("sp", None),
            P("sp"),
            P("sp", None),
            P("sp", "tp", None),
            P("sp", "tp", None),
            P("sp", "tp", None),
            P("tp", "sp"),
            P("tp", "sp"),
            P("tp", "sp"),
            P("tp", "sp"),
            P(None, "tp"),
            P(None, "tp"),
        ),
        out_specs=(
            P("sp", "tp"),
            P("sp", "tp", None),
            P("sp", "tp", None),
            P("sp", "tp", None),
            P("sp", "tp"),
            P("tp", "sp"),
            P("tp", "sp"),
            P("tp", "sp"),
        ),
        check_vma=False,
    )
```

profile of v0, /device:TPU:0, one launch (start us, length us, event | category | flops | bytes accessed | tf_op | source)
XLA Modules:
  0.0 227.4 jit_solution(1692050622899600530)
XLA Ops:
  7.2 0.8 broadcast_multiply_fusion.1
  8.0 0.7 broadcast_multiply_fusion
  9.1 0.6 reduce-window.6
  9.7 0.2 slice_reduce_fusion
  10.1 0.1 mul.119
  10.3 1.4 scatter_custom_fusion
  11.9 0.9 constant_dynamic-slice_fusion
  12.8 2.1 gather_fusion.2
  15.1 20.4 %all_to_all.15 = bf16[8,52,512]{2,1,0:T(8,128)(2,1)} all-to-all(bf16[8,52,512]{2,1,0:T(8,128)(2,1)S(1)} %broadcast_select_fusion), channel_id=1, replica_groups=mesh['sp'=8,'tp'=4] {'sp'}, dimensions={0} | all-to-all | bytes 851968 | tf_op jit(solution)/shard_map/all_to_all | solution.py:70
  35.6 0.9 constant_dynamic-slice_fusion.1
  36.5 2.1 gather_fusion.1
  39.0 3.2 %gather_fusion = f32[416]{0:T(512)S(1)} fusion(f32[256]{0:T(256)S(1)} %reshape.111, s32[1024]{0:T(1024)S(1)} %get-tuple-element.40), kind=kCustom, calls=%fused_computation | custom fusion | bytes 4992 | tf_op jit(solution)/shard_map/gather | solution.py:18
  42.3 0.2 select_convert_fusion
  42.5 16.4 %all_to_all.16 = bf16[8,52,512]{2,1,0:T(8,128)(2,1)} all-to-all(bf16[8,52,512]{2,1,0:T(8,128)(2,1)S(1)} %select_convert_fusion), channel_id=1, replica_groups=mesh['sp'=8,'tp'=4] {'sp'}, dimensions={0} | all-to-all | bytes 851968 | tf_op jit(solution)/shard_map/all_to_all | solution.py:71
  59.0 2.5 %reshape.113 = bf16[416,2048]{1,0:T(8,128)(2,1)} reshape(bf16[8,52,2048]{2,1,0:T(8,128)(2,1)} %all-gather.5.cloned.1.call-done) | data formatting | bytes 3407872 | tf_op jit(solution)/shard_map/reshape | solution.py:77
  61.5 2.7 %fusion.5 = f32[416,512]{1,0:T(8,128)S(1)} fusion(bf16[416,2048]{1,0:T(8,128)(2,1)} %reshape.113, bf16[1,512,2048]{2,1,0:T(8,128)(2,1)S(1)} %copy-done), kind=kOutput, calls=%fused_computation.15 | convolution fusion | flops 872415232 | bytes 4653056 | tf_op jit(solution)/shard_map/dot_general | solution.py:84
  64.2 2.0 fusion.8
  66.2 12.9 %all-gather.3.cloned.1.call-done = bf16[8,52,2048]{2,1,0:T(8,128)(2,1)} async-done(((bf16[8,52,512]{2,1,0:T(8,128)(2,1)}), bf16[8,52,2048]{2,1,0:T(8,128)(2,1)}) %all-gather.3.cloned.1.call-update) | async-done | bytes 1703952 | tf_op jit(solution)/shard_map/all_gather | solution.py:75
  79.1 2.5 %reshape.112 = bf16[416,2048]{1,0:T(8,128)(2,1)} reshape(bf16[8,52,2048]{2,1,0:T(8,128)(2,1)} %all-gather.3.cloned.1.call-done) | data formatting | bytes 3407872 | tf_op jit(solution)/shard_map/reshape | solution.py:78
  81.6 3.6 %multiply_convert_fusion.1 = (bf16[416,512]{1,0:T(8,128)(2,1)S(1)}, bf16[416,512]{1,0:T(8,128)(2,1)S(1)}) fusion(f32[416,512]{1,0:T(8,128)S(1)} %fusion.5, f32[416,512]{1,0:T(8,128)} %fusion.8, bf16[416,2048]{1,0:T(8,128)(2,1)} %reshape.112, bf16[1,512,2048]{2,1,0:T(8,128)(2,1)} %param.23), kind=kOutput, calls=%fused_computation.25 | convolution fusion | flops 875184128 | bytes 6356992 | tf_op jit(solution)/shard_map/dot_general | solution.py:86
  85.2 1.0 fusion.3
  86.3 0.7 copy-done.3
  86.9 2.2 add_convert_fusion
  89.2 28.9 %reduce-scatter.3.cloned.1.call-done = bf16[416,512]{1,0:T(8,128)(2,1)} async-done(((bf16[416,2048]{1,0:T(8,128)(2,1)}), bf16[416,512]{1,0:T(8,128)(2,1)}) %reduce-scatter.3.cloned.1.call-update) | async-done | bytes 426000 | tf_op jit(solution)/shard_map/reduce_scatter | solution.py:106
  118.1 1.9 reshape.114
  120.0 5.5 %all-to-all-start.2 = ((bf16[8,52,512]{2,1,0:T(8,128)(2,1)}), bf16[8,52,512]{2,1,0:T(8,128)(2,1)S(1)}, u32[]{:S(2)}, u32[]{:S(2)}) async-start(bf16[8,52,512]{2,1,0:T(8,128)(2,1)} %reshape.114), calls=%async_computation.3 | async-start | bytes 917504 | tf_op jit(solution)/shard_map/all_to_all | solution.py:109
  125.7 0.8 copy.37
  126.5 12.0 %all-to-all-done.2 = bf16[8,52,512]{2,1,0:T(8,128)(2,1)S(1)} async-done(((bf16[8,52,512]{2,1,0:T(8,128)(2,1)}), bf16[8,52,512]{2,1,0:T(8,128)(2,1)S(1)}, u32[]{:S(2)}, u32[]{:S(2)}) %all-to-all-start.2) | async-done | bytes 426016 | tf_op jit(solution)/shard_map/all_to_all | solution.py:109
  138.5 1.9 gather_fusion.3
  140.4 1.3 reshape.117
  141.7 0.4 fusion.35
  142.1 1.0 fusion.21
  143.1 6.7 %all_gather.11 = bf16[128,2048]{1,0:T(8,128)(2,1)S(1)} all-gather(bf16[128,512]{1,0:T(8,128)(2,1)S(1)} %fusion.21), channel_id=1, replica_groups=mesh['sp'=8,'tp'=4] {'tp'}, dimensions={1}, use_global_device_ids=true | all-gather | bytes 655360 | tf_op jit(solution)/shard_map/all_gather | solution.py:117
  149.8 2.1 convolution_convert_fusion
  151.9 1.0 copy.39
  152.9 1.7 copy.38
  154.6 4.3 %fusion = bf16[1,512,2048]{2,1,0:T(8,128)(2,1)} fusion(bf16[416,512]{1,0:T(8,128)(2,1)} %copy-done.10, bf16[416,2048]{1,0:T(8,128)(2,1)} %reshape.113), kind=kOutput, calls=%fused_computation.10 | convolution fusion | flops 873463808 | bytes 4227072 | tf_op jit(solution)/shard_map/dot_general | solution.py:97
  159.0 2.7 %fusion.2 = bf16[1,512,2048]{2,1,0:T(8,128)(2,1)} fusion(bf16[416,2048]{1,0:T(8,128)(2,1)S(1)} %copy-done.6, f32[416,512]{1,0:T(8,128)S(1)} %copy-done.21, f32[416,512]{1,0:T(8,128)S(1)} %copy-done.20), kind=kOutput, calls=%fused_computation.12 | convolution fusion | flops 874741760 | bytes 5505024 | tf_op jit(solution)/shard_map/dot_general | solution.py:103
  161.7 1.1 convert_multiply_fusion.2
  162.8 0.7 copy-done.8
  163.5 1.4 collective-permute-start
  165.0 2.6 %fusion.1 = bf16[1,512,2048]{2,1,0:T(8,128)(2,1)} fusion(bf16[416,512]{1,0:T(8,128)(2,1)S(1)} %get-tuple-element.28, bf16[416,2048]{1,0:T(8,128)(2,1)S(1)} %copy-done.5), kind=kOutput, calls=%fused_computation.11 | convolution fusion | flops 873463808 | bytes 4227072 | tf_op jit(solution)/shard_map/dot_general | solution.py:100
  167.6 0.8 copy.40
  168.4 0.8 collective-permute-done
  169.3 0.8 copy.41
  170.1 0.8 copy.42
  170.8 48.2 %reduce-scatter.5.cloned.1.call-done = bf16[256,512]{1,0:T(8,128)(2,1)} async-done(((bf16[2048,512]{1,0:T(8,128)(2,1)}), bf16[256,512]{1,0:T(8,128)(2,1)}) %reduce-scatter.5.cloned.1.call-update) | async-done | bytes 262160 | tf_op jit(solution)/shard_map/reduce_scatter | solution.py:122
  219.1 1.8 convert_element_type.103
  (81 shorter events, 2.1 us)
Async XLA Ops:
  7.2 54.3 %copy-start = (bf16[1,512,2048]{2,1,0:T(8,128)(2,1)S(1)}, bf16[1,512,2048]{2,1,0:T(8,128)(2,1)}, u32[]{:S(2)}) copy-start(bf16[1,512,2048]{2,1,0:T(8,128)(2,1)} %param.21) | copy-start | bytes 6291460
  7.2 51.8 %all-gather.5.cloned.1.call-start = ((), (), s32[]{:S(2)}) async-start(), calls=%async_computation.6 | async-start | bytes 2293760 | tf_op jit(solution)/shard_map/all_gather | solution.py:74
  35.5 43.6 %all-gather.3.cloned.1.call-start = ((), (), s32[]{:S(2)}) async-start(), calls=%async_computation.5 | async-start | bytes 2293760 | tf_op jit(solution)/shard_map/all_gather | solution.py:75
  36.5 2.2 copy-start.16
  36.5 2.2 copy-start.18
  58.9 59.3 %reduce-scatter.3.cloned.1.call-start = ((), (), s32[]{:S(2)}) async-start(), calls=%async_computation.7 | async-start | bytes 2129920 | tf_op jit(solution)/shard_map/reduce_scatter | solution.py:106
  61.5 2.7 %copy-start.2 = (bf16[1,512,2048]{2,1,0:T(8,128)(2,1)S(1)}, bf16[1,512,2048]{2,1,0:T(8,128)(2,1)}, u32[]{:S(2)}) copy-start(bf16[1,512,2048]{2,1,0:T(8,128)(2,1)} %param.22) | copy-start | bytes 6291460
  61.5 2.7 %copy-start.4 = (bf16[416,2048]{1,0:T(8,128)(2,1)S(1)}, bf16[416,2048]{1,0:T(8,128)(2,1)}, u32[]{:S(2)}) copy-start(bf16[416,2048]{1,0:T(8,128)(2,1)} %reshape.113) | copy-start | bytes 5111812
  64.2 17.4 %copy-start.19 = (f32[416,512]{1,0:T(8,128)}, f32[416,512]{1,0:T(8,128)S(1)}, u32[]{:S(2)}) copy-start(f32[416,512]{1,0:T(8,128)S(1)} %fusion.5) | copy-start | bytes 2555908
  85.2 1.1 copy-start.10
  85.2 1.7 copy-start.3
  89.2 36.4 %copy-start.14 = (bf16[512,128]{1,0:T(8,128)(2,1)S(1)}, bf16[512,128]{1,0:T(8,128)(2,1)}, u32[]{:S(2)}) copy-start(bf16[512,128]{1,0:T(8,128)(2,1)} %param.24) | copy-start | bytes 393220
  89.2 36.5 %copy-start.15 = (bf16[512,128]{1,0:T(8,128)(2,1)S(1)}, bf16[512,128]{1,0:T(8,128)(2,1)}, u32[]{:S(2)}) copy-start(bf16[512,128]{1,0:T(8,128)(2,1)} %param.27) | copy-start | bytes 393220
  120.0 18.4 %all-to-all-start.2 = ((bf16[8,52,512]{2,1,0:T(8,128)(2,1)}), bf16[8,52,512]{2,1,0:T(8,128)(2,1)S(1)}, u32[]{:S(2)}, u32[]{:S(2)}) async-start(bf16[8,52,512]{2,1,0:T(8,128)(2,1)} %reshape.114), calls=%async_computation.3 | async-start | bytes 917504 | tf_op jit(solution)/shard_map/all_to_all | solution.py:109
  125.5 93.5 %reduce-scatter.5.cloned.1.call-start = ((), (), s32[]{:S(2)}) async-start(), calls=%async_computation.8 | async-start | bytes 2359296 | tf_op jit(solution)/shard_map/reduce_scatter | solution.py:122
  140.4 9.4 %copy-start.7 = (bf16[512,128]{0,1:T(8,128)(2,1)S(1)}, bf16[512,128]{0,1:T(8,128)(2,1)}, u32[]{:S(2)}) copy-start(bf16[512,128]{0,1:T(8,128)(2,1)} %copy.37) | copy-start | bytes 393220
  143.1 8.8 %copy-start.12 = (bf16[128,512]{1,0:T(8,128)(2,1)}, bf16[128,512]{1,0:T(8,128)(2,1)S(1)}, u32[]{:S(2)}) copy-start(bf16[128,512]{1,0:T(8,128)(2,1)S(1)} %fusion.21) | copy-start | bytes 393220
  149.8 4.8 %copy-start.17 = (f32[3,512]{1,0:T(4,128)S(1)}, f32[3,512]{1,0:T(4,128)}, u32[]{:S(2)}) copy-start(f32[3,512]{1,0:T(4,128)} %param.28) | copy-start | bytes 18436
  154.6 4.4 %copy-start.6 = (bf16[416,2048]{1,0:T(8,128)(2,1)S(1)}, bf16[416,2048]{1,0:T(8,128)(2,1)}, u32[]{:S(2)}) copy-start(bf16[416,2048]{1,0:T(8,128)(2,1)} %reshape.112) | copy-start | bytes 5111812
  154.6 4.4 %copy-start.20 = (f32[416,512]{1,0:T(8,128)S(1)}, f32[416,512]{1,0:T(8,128)}, u32[]{:S(2)}) copy-start(f32[416,512]{1,0:T(8,128)} %copy-done.19) | copy-start | bytes 2555908
  154.6 4.3 %copy-start.21 = (f32[416,512]{1,0:T(8,128)S(1)}, f32[416,512]{1,0:T(8,128)}, u32[]{:S(2)}) copy-start(f32[416,512]{1,0:T(8,128)} %fusion.8) | copy-start | bytes 2555908
  159.0 2.7 %copy-start.1 = (bf16[2048,512]{1,0:T(8,128)(2,1)S(1)}, bf16[2048,512]{1,0:T(8,128)(2,1)}, u32[]{:S(2)}) copy-start(bf16[2048,512]{1,0:T(8,128)(2,1)} %param.29) | copy-start | bytes 6291460
  161.7 3.3 %copy-start.5 = (bf16[416,2048]{1,0:T(8,128)(2,1)S(1)}, bf16[416,2048]{1,0:T(8,128)(2,1)}, u32[]{:S(2)}) copy-start(bf16[416,2048]{1,0:T(8,128)(2,1)} %reshape.113) | copy-start | bytes 5111812
  162.8 0.7 copy-start.8
  163.5 4.1 %copy-start.11 = (bf16[512,128]{0,1:T(8,128)(2,1)S(1)}, bf16[512,128]{0,1:T(8,128)(2,1)}, u32[]{:S(2)}) copy-start(bf16[512,128]{0,1:T(8,128)(2,1)} %get-tuple-element.33) | copy-start | bytes 393220
  163.5 5.6 %copy-start.9 = (f32[512,128]{0,1:T(8,128)S(1)}, f32[512,128]{0,1:T(8,128)}, u32[]{:S(2)}) copy-start(f32[512,128]{0,1:T(8,128)} %copy-done.8) | copy-start | bytes 786436
  163.5 5.8 %copy-start.13 = (bf16[512,128]{0,1:T(8,128)(2,1)S(1)}, bf16[512,128]{0,1:T(8,128)(2,1)}, u32[]{:S(2)}) copy-start(bf16[512,128]{0,1:T(8,128)(2,1)} %copy.38) | copy-start | bytes 393220
  163.5 5.6 %collective-permute-start = (f32[512,2]{0,1:T(2,128)S(1)}, f32[512,2]{0,1:T(2,128)S(1)}, u32[]{:S(2)}, u32[]{:S(2)}) collective-permute-start(f32[512,2]{0,1:T(2,128)S(1)} %slice.51), channel_id=1, source_target_pairs={{4,0},{8,4},{12,8},{16,12},{20,16},{24,20},{28,24},{5,1},{9,5},{13... | collective-permute-start | bytes 12296 | tf_op jit(solution)/shard_map/ppermute | solution.py:13
Sparse Core Ops, SparseCore 0:
  35.6 20.0 all-gather.4
  59.0 20.0 all-gather.2
  89.3 28.7 reduce-scatter.2
  152.0 66.9 reduce-scatter.4
where the time goes:
time: 228 us; the launch traced here: 227 us
  waiting for transfers between devices  103 us (45%)
  blocking collectives  43.5 us (19%)
  local copies, waits for them, and re-layouts  29.9 us (13%)
  matrix products  24.4 us (11%)
  between operations  14.2 us (6%)
  starting transfers between devices  7.09 us (3%)
  other arithmetic  5.52 us (2%)
    reduce_scatter x1, waiting for transfers between devices, per_device(): lax.psum_scatter(lax.dot_general(grad_rows, mixer_out, (((0,), (1,)), (()...  48.2 us
    reduce_scatter x1, waiting for transfers between devices, per_device(): lax.psum_scatter(partial_rows.astype(jnp.bfloat16), 'tp', scatter_dimensi...  28.9 us
    all_to_all x1, blocking collectives, per_device(): lax.all_to_all(input_send, 'sp', split_axis=0, concat_axis=0, tiled=True)  20.4 us
    all_to_all x1, blocking collectives, per_device(): lax.all_to_all(scaled_send, 'sp', split_axis=0, concat_axis=0, tiled=True)  16.4 us
    all_gather x1, waiting for transfers between devices, per_device(): lax.all_gather(scaled_part, 'tp', axis=2, tiled=True)  12.9 us
    all_to_all x1, waiting for transfers between devices, per_device(): lax.all_to_all(shares.reshape(experts, capacity, col_piece), 'sp', split_...  12 us
    unnamed x51, local copies, waits for them, and re-layouts  7.31 us
    all_gather x1, blocking collectives, per_device(): grad_rows = lax.all_gather(own_cols, 'tp', axis=1, tiled=True)  6.68 us
  transfers between devices with their start and end apart: 6, of which 5 were waited for; matrix products, arithmetic and copies ran while one was open for 14% of the time, Pallas kernels for 0%

commit v1 on v0

--- a/solution.py
+++ b/solution.py
@@ -1,10 +1,249 @@
+import functools
+
 import jax
 import jax.numpy as jnp
 from jax import lax
+from jax.experimental import pallas as pl
+from jax.experimental.pallas import tpu as pltpu
 from jax.sharding import PartitionSpec as P
 
 TAPS = 3
 INNER = 4
+
+
+MESH = pl.DeviceIdType.MESH
+
+
+def places(experts, rows):
+    me, tp = lax.axis_index("sp"), lax.axis_index("tp")
+    return me, tp // 2, lax.rem(tp, 2)
+
+
+def greet(experts, rows):
+    me, y, core = places(experts, rows)
+    barrier = pltpu.get_barrier_semaphore()
+    for step in range(1, experts):
+        pl.semaphore_signal(
+            barrier, inc=1, device_id={"sp": lax.rem(me + step, experts)}, device_id_type=MESH
+        )
+    for step in range(1, rows):
+        pl.semaphore_signal(
+            barrier,
+            inc=1,
+            device_id={"tp": lax.rem(y + step, rows) * 2 + core},
+            device_id_type=MESH,
+        )
+    pl.semaphore_signal(barrier, inc=1, device_id={"tp": y * 2 + 1 - core}, device_id_type=MESH)
+    pl.semaphore_wait(barrier, experts + rows - 1)
+
+
+def dispatch_kernel(
+    experts, rows, x_ref, out_ref, s_sem, r_sem, ys_sem, yr_sem, ps_sem, pr_sem
+):
+    me, y, core = places(experts, rows)
+    width = x_ref.shape[-1]
+
+    def block(source, row, side):
+        column = pl.multiple_of((row * 2 + side) * width, width)
+        return out_ref.at[:, source, :, pl.ds(column, width)]
+
+    def across(step):
+        target = lax.rem(me + step, experts)
+        return pltpu.make_async_remote_copy(
+            src_ref=x_ref.at[:, target],
+            dst_ref=block(me, y, core),
+            send_sem=s_sem.at[step],
+            recv_sem=r_sem.at[step],
+            device_id={"sp": target},
+            device_id_type=MESH,
+        )
+
+    def to_row(hop, step, own):
+        source = lax.rem(me - step + experts, experts)
+        return pltpu.make_async_remote_copy(
+            src_ref=x_ref.at[:, me] if own else block(source, y, core),
+            dst_ref=block(source, y, core),
+            send_sem=ys_sem.at[hop, step],
+            recv_sem=yr_sem.at[hop, step],
+            device_id={"tp": lax.rem(y + hop, rows) * 2 + core},
+            device_id_type=MESH,
+        )
+
+    def to_partner(hop, step, own):
+        source = lax.rem(me - step + experts, experts)
+        row = lax.rem(y - hop + rows, rows)
+        return pltpu.make_async_remote_copy(
+            src_ref=x_ref.at[:, me] if own else block(source, row, core),
+            dst_ref=block(source, row, core),
+            send_sem=ps_sem.at[hop, step],
+            recv_sem=pr_sem.at[hop, step],
+            device_id={"tp": y * 2 + 1 - core},
+            device_id_type=MESH,
+        )
+
+    def loop(start, body):
+        lax.fori_loop(start, experts, lambda step, carry: (body(step), carry)[1], 0)
+
+    greet(experts, rows)
+    for hop in range(1, rows):
+        to_row(hop, 0, True).start()
+    loop(1, lambda step: across(step).start())
+    to_partner(0, 0, True).start()
+    own_column = pl.multiple_of((y * 2 + core) * width, width)
+    for kind in range(x_ref.shape[0]):
+        out_ref[kind, me, :, pl.ds(own_column, width)] = x_ref[kind, me]
+
+    def forward(step):
+        across(step).wait_recv()
+        for hop in range(1, rows):
+            to_row(hop, step, False).start()
+        to_partner(0, step, False).start()
+        for hop in range(1, rows):
+            to_row(hop, step - 1, False).wait_recv()
+            to_partner(hop, step - 1, False).start()
+
+    loop(1, forward)
+    for hop in range(1, rows):
+        to_row(hop, experts - 1, False).wait_recv()
+        to_partner(hop, experts - 1, False).start()
+
+    def finish(step):
+        for hop in range(rows):
+            to_partner(hop, step, False).wait()
+        for hop in range(1, rows):
+            to_row(hop, step, False).wait_send()
+
+    loop(0, finish)
+    loop(1, lambda step: across(step).wait_send())
+
+
+def dispatch(packed, experts, rows):
+    kinds, _, slots, width = packed.shape
+    dma = pltpu.SemaphoreType.DMA
+    return pl.pallas_call(
+        functools.partial(dispatch_kernel, experts, rows),
+        out_shape=jax.ShapeDtypeStruct((kinds, experts, slots, 2 * rows * width), packed.dtype),
+        in_specs=[pl.BlockSpec(memory_space=pltpu.VMEM)],
+        out_specs=pl.BlockSpec(memory_space=pltpu.VMEM),
+        scratch_shapes=[dma((experts,))] * 2 + [dma((rows, experts))] * 4,
+        compiler_params=pltpu.CompilerParams(collective_id=0, has_side_effects=True),
+    )(packed)
+
+
+def combine_kernel(
+    experts,
+    rows,
+    x_ref,
+    out_ref,
+    from_partner,
+    row_out,
+    row_in,
+    total,
+    ps_sem,
+    pr_sem,
+    ys_sem,
+    yr_sem,
+    s_sem,
+    r_sem,
+):
+    me, y, core = places(experts, rows)
+    width = out_ref.shape[-1]
+
+    def columns(row, side):
+        return pl.ds(pl.multiple_of((row * 2 + side) * width, width), width)
+
+    def to_partner(hop):
+        row = lax.rem(y + hop, rows)
+        return pltpu.make_async_remote_copy(
+            src_ref=x_ref.at[:, :, columns(row, 1 - core)],
+            dst_ref=from_partner.at[hop],
+            send_sem=ps_sem.at[hop],
+            recv_sem=pr_sem.at[hop],
+            device_id={"tp": y * 2 + 1 - core},
+            device_id_type=MESH,
+        )
+
+    def to_row(hop, step):
+        return pltpu.make_async_remote_copy(
+            src_ref=row_out.at[hop, step],
+            dst_ref=row_in.at[hop, step],
+            send_sem=ys_sem.at[hop, step],
+            recv_sem=yr_sem.at[hop, step],
+            device_id={"tp": lax.rem(y + hop, rows) * 2 + core},
+            device_id_type=MESH,
+        )
+
+    def across(step):
+        return pltpu.make_async_remote_copy(
+            src_ref=total.at[step],
+            dst_ref=out_ref.at[me],
+            send_sem=s_sem.at[step],
+            recv_sem=r_sem.at[step],
+            device_id={"sp": lax.rem(me + step, experts)},
+            device_id_type=MESH,
+        )
+
+    def pair(hop, step):
+        target = lax.rem(me + step, experts)
+        own = x_ref[target, :, columns(lax.rem(y + hop, rows), core)].astype(jnp.float32)
+        return own + from_partner[hop, target].astype(jnp.float32)
+
+    def loop(start, body):
+        lax.fori_loop(start, experts, lambda step, carry: (body(step), carry)[1], 0)
+
+    def send_row(hop, step):
+        row_out[hop, step] = pair(hop, step).astype(jnp.bfloat16)
+        to_row(hop, step).start()
+
+    def whole(step):
+        value = pair(0, step)
+        for hop in range(1, rows):
+            to_row(hop, step).wait_recv()
+            value = value + row_in[hop, step].astype(jnp.float32)
+        return value.astype(jnp.bfloat16)
+
+    def send_across(step):
+        total[step] = whole(step)
+        across(step).start()
+
+    greet(experts, rows)
+    for hop in [*range(1, rows), 0]:
+        to_partner(hop).start()
+    for hop in range(1, rows):
+        to_partner(hop).wait_recv()
+        loop(1, functools.partial(send_row, hop))
+        send_row(hop, 0)
+    to_partner(0).wait_recv()
+    loop(1, send_across)
+    out_ref[me] = whole(0)
+
+    def finish(step):
+        for hop in range(1, rows):
+            to_row(hop, step).wait_send()
+
+    loop(0, finish)
+    loop(1, lambda step: across(step).wait())
+    for hop in range(rows):
+        to_partner(hop).wait_send()
+
+
+def combine(partial, experts, rows):
+    _, slots, full = partial.shape
+    width = full // (2 * rows)
+    dma = pltpu.SemaphoreType.DMA
+    held = pltpu.VMEM((rows, experts, slots, width), partial.dtype)
+    return pl.pallas_call(
+        functools.partial(combine_kernel, experts, rows),
+        out_shape=jax.ShapeDtypeStruct((experts, slots, width), partial.dtype),
+        in_specs=[pl.BlockSpec(memory_space=pltpu.VMEM)],
+        out_specs=pl.BlockSpec(memory_space=pltpu.VMEM),
+        scratch_shapes=[held] * 3
+        + [pltpu.VMEM((experts, slots, width), partial.dtype)]
+        + [dma((rows,))] * 2
+        + [dma((rows, experts))] * 2
+        + [dma((experts,))] * 2,
+        compiler_params=pltpu.CompilerParams(collective_id=1, has_side_effects=True),
+    )(partial)
 
 
 def from_behind(value, axis, steps):
@@ -44,6 +283,10 @@
     column = lax.axis_index("tp") * col_piece
     group_count = experts // INNER
     capacity = 4 * (3 * tok_rows // (16 * group_count) + 1)
+    capacity = -(-capacity // 8) * 8
+    tp_rows = lax.axis_size("tp") // 2
+    mixer_out = (outer_gate.astype(jnp.float32) * conv_out.astype(jnp.float32)).astype(jnp.bfloat16)
+    mixer_all = lax.all_gather(mixer_out.T, "sp", axis=0, tiled=True)
     entry_count = 2 * tok_rows
     expert_ids = (INNER * group_choice[:, None] + inner_pair).reshape(-1)
     onehot = (expert_ids[:, None] == jnp.arange(experts, dtype=jnp.int32)[None, :]).astype(
@@ -66,16 +309,9 @@
     input_send, scaled_send = pack_rows(
         input_cols, cot_cols, token_of, entry_of, filled, routing_flat, experts, capacity
     )
-    input_part, scaled_part = (
-        lax.all_to_all(input_send, "sp", split_axis=0, concat_axis=0, tiled=True),
-        lax.all_to_all(scaled_send, "sp", split_axis=0, concat_axis=0, tiled=True),
-    )
-    input_recv, scaled_recv = (
-        lax.all_gather(input_part, "tp", axis=2, tiled=True),
-        lax.all_gather(scaled_part, "tp", axis=2, tiled=True),
-    )
-    in_rows = input_recv.reshape(-1, model_width)
-    scaled_rows = scaled_recv.reshape(-1, model_width)
+    received = dispatch(jnp.stack([input_send, scaled_send]), experts, tp_rows)
+    in_rows = received[0].reshape(-1, model_width)
+    scaled_rows = received[1].reshape(-1, model_width)
     gate_weight = w_gate[0]
     up_weight = w_up[0]
     down_weight = w_down[0]
@@ -103,11 +339,8 @@
     grad_w_down = lax.dot_general(
         hidden, scaled_rows, row_dims, preferred_element_type=jnp.float32
     ).astype(jnp.bfloat16)
-    shares = lax.psum_scatter(
-        partial_rows.astype(jnp.bfloat16), "tp", scatter_dimension=1, tiled=True
-    )
-    returned = lax.all_to_all(
-        shares.reshape(experts, capacity, col_piece), "sp", split_axis=0, concat_axis=0, tiled=True
+    returned = combine(
+        partial_rows.astype(jnp.bfloat16).reshape(experts, capacity, model_width), experts, tp_rows
     )
     back_tok = (
         returned.reshape(-1, col_piece)[target].reshape(tok_rows, 2, col_piece).astype(jnp.float32)
@@ -118,15 +351,8 @@
     grad_out = lax.dot_general(
         w_out, grad_rows, (((0,), (1,)), ((), ())), preferred_element_type=jnp.float32
     )
-    mixer_out = (outer_gate.astype(jnp.float32) * conv_out.astype(jnp.float32)).astype(jnp.bfloat16)
-    grad_w_out = lax.psum_scatter(
-        lax.dot_general(
-            grad_rows, mixer_out, (((0,), (1,)), ((), ())), preferred_element_type=jnp.float32
-        ).astype(jnp.bfloat16),
-        "sp",
-        scatter_dimension=0,
-        tiled=True,
-    ).astype(jnp.float32)
+    grad_all = lax.all_to_all(grad_rows, "sp", split_axis=1, concat_axis=0, tiled=True)
+    grad_w_out = lax.dot_general(grad_all, mixer_all, row_dims, preferred_element_type=jnp.float32)
     grad_outer_gate = (grad_out * conv_out.astype(jnp.float32)).astype(jnp.bfloat16)
     grad_conv = grad_out * outer_gate.astype(jnp.float32)
     following = from_behind(grad_conv[:, : TAPS - 1], "sp", -1)

time: 228 us -> 173 us (0.76)
  waiting for transfers between devices: 103 us -> 23.8 us
  Pallas kernels: 0 us -> 65.6 us
  blocking collectives: 43.5 us -> 6.68 us
  local copies, waits for them, and re-layouts: 29.9 us -> 25.8 us
  matrix products: 24.4 us -> 22 us
    reduce_scatter x2 -> x0, waiting for transfers between devices: 77.2 us -> none  [the longest x1 48.2 us: per_device(): lax.psum_scatter(lax.dot_general(grad_rows, mixer_out, (((0,), (1,)), (()...]
    pallas_call x0 -> x2, Pallas kernels: none -> 65.6 us  [the longest x1 38.3 us: dispatch(): pl.pallas_call(functools.partial(dispatch_kernel, experts, rows), out_sha...]
    all_to_all x2 -> x0, blocking collectives: 36.8 us -> none  [the longest x1 20.4 us: per_device(): lax.all_to_all(input_send, 'sp', split_axis=0, concat_axis=0, tiled=True)]
    reshape x4 -> x0, local copies, waits for them, and re-layouts: 6.98 us -> none  [the longest x1 2.53 us: per_device(): in_rows = input_recv.reshape(-1, model_width)]
    all_to_all x1, waiting for transfers between devices: 12 us -> 6.56 us  [per_device(): lax.all_to_all(grad_rows, 'sp', split_axis=1, concat_axis=0, tiled=True)]
    all_gather x2 -> x1, waiting for transfers between devices: 12.9 us -> 17.3 us  [per_device(): mixer_all = lax.all_gather(mixer_out.T, 'sp', axis=0, tiled=True)]
    slice x1 -> x2, local copies, waits for them, and re-layouts: 0.21 us -> 2.75 us  [the longest x1 2.54 us: per_device(): scaled_rows = received[1].reshape(-1, model_width)]
    unnamed x51 -> x43, local copies, waits for them, and re-layouts: 7.31 us -> 8.37 us
  transfers between devices with their start and end apart: 6 -> 3, of which waited for: 5 -> 2; matrix products, arithmetic and copies ran while one was open for 14% -> 8% of each run, Pallas kernels for 0% -> 0%
where the time goes in v1:
time: 173 us; the launch traced here: 172 us
  Pallas kernels  65.6 us (38%)
  local copies, waits for them, and re-layouts  25.8 us (15%)
  waiting for transfers between devices  23.8 us (14%)
  matrix products  22 us (13%)
  between operations  14.5 us (8%)
  starting transfers between devices  7.85 us (5%)
  blocking collectives  6.68 us (4%)
  other arithmetic  5.84 us (3%)
    pallas_call x1, Pallas kernels, dispatch(): pl.pallas_call(functools.partial(dispatch_kernel, experts, rows), out_sha...  38.3 us
    pallas_call x1, Pallas kernels, combine(): pl.pallas_call(functools.partial(combine_kernel, experts, rows), out_shap...  27.3 us
    all_gather x1, waiting for transfers between devices, per_device(): mixer_all = lax.all_gather(mixer_out.T, 'sp', axis=0, tiled=True)  17.3 us
    unnamed x43, local copies, waits for them, and re-layouts  8.37 us
    all_gather x1, blocking collectives, per_device(): grad_rows = lax.all_gather(own_cols, 'tp', axis=1, tiled=True)  6.68 us
    all_to_all x1, waiting for transfers between devices, per_device(): lax.all_to_all(grad_rows, 'sp', split_axis=1, concat_axis=0, tiled=True)  6.56 us
    all_to_all x1, starting transfers between devices, per_device(): lax.all_to_all(grad_rows, 'sp', split_axis=1, concat_axis=0, tiled=True)  6.52 us
    dot_general x1, matrix products, per_device(): lax.dot_general(grad_up, in_rows, row_dims, preferred_element_type=jnp.fl...  4.27 us
  transfers between devices with their start and end apart: 3, of which 2 were waited for; matrix products, arithmetic and copies ran while one was open for 8% of the time, Pallas kernels for 0%

profile of v1, /device:TPU:0, one launch (start us, length us, event | category | flops | bytes accessed | tf_op | source)
XLA Modules:
  0.0 172.2 jit_solution(18092848887468544120)
XLA Ops:
  7.2 0.8 broadcast_multiply_fusion.1
  8.0 0.7 broadcast_multiply_fusion
  8.8 0.1 eq.29
  9.0 0.1 eq.25
  9.1 0.6 reduce-window.6
  9.7 0.2 slice_reduce_fusion
  10.1 0.1 mul.125
  10.3 1.4 scatter_custom_fusion
  11.8 0.7 reduce_max.9
  12.5 0.7 fusion.34
  13.2 0.7 divide_multiply_fusion
  14.0 0.1 reshape.139
  14.2 3.2 %gather_fusion.1 = f32[448]{0:T(512)S(1)} fusion(f32[256]{0:T(256)S(1)} %reshape.139, s32[1024]{0:T(1024)S(1)} %get-tuple-element.44), kind=kCustom, calls=%fused_computation.1 | custom fusion | bytes 5376 | tf_op jit(solution)/shard_map/gather | solution.py:257
  17.5 1.0 constant_dynamic-slice_fusion
  18.5 2.1 %gather_fusion.2 = bf16[448,512]{1,0:T(8,128)(2,1)S(1)} fusion(bf16[128,512]{1,0:T(8,128)(2,1)S(1)} %get-tuple-element.43, s32[1024]{0:T(1024)S(1)} %get-tuple-element.45), kind=kCustom, calls=%fused_computation.2 | custom fusion | bytes 919296 | tf_op jit(solution)/shard_map/gather | solution.py:257
  20.6 2.1 %gather_fusion = bf16[448,512]{1,0:T(8,128)(2,1)S(1)} fusion(bf16[128,512]{1,0:T(8,128)(2,1)S(1)} %get-tuple-element.42, s32[1024]{0:T(1024)S(1)} %get-tuple-element.45), kind=kCustom, calls=%fused_computation | custom fusion | bytes 919296 | tf_op jit(solution)/shard_map/gather | solution.py:256
  22.7 0.1 broadcast_select_fusion
  22.8 0.2 fusion.13
  23.0 1.0 pad_maximum_fusion.x_ref
  24.0 38.3 %shard_map.206 = bf16[2,8,56,2048]{3,2,1,0:T(8,128)(2,1)} custom-call(bf16[2,8,56,512]{3,2,1,0:T(8,128)(2,1)} %pad_maximum_fusion.x_ref), custom_call_target="tpu_custom_call" | custom-call | tf_op jit(solution)/shard_map/pallas_call | solution.py:123
  62.4 2.5 %fusion.37 = (bf16[1,8,56,2048]{3,2,1,0:T(8,128)(2,1)S(1)}, bf16[1,8,56,2048]{3,2,1,0:T(8,128)(2,1)S(1)}) fusion(bf16[2,8,56,2048]{3,2,1,0:T(8,128)(2,1)} %shard_map.206), kind=kLoop, calls=%fused_computation.86 | loop fusion | bytes 7340032 | tf_op jit(solution)/shard_map/slice | solution.py:314
  64.9 1.1 fusion.5
  66.1 1.7 copy-done.1
  67.8 1.2 fusion.8
  69.1 0.7 copy-done.13
  69.8 1.4 multiply_convert_fusion.1
  71.2 1.1 fusion.3
  72.4 2.4 %add_convert_fusion = bf16[448,2048]{1,0:T(8,128)(2,1)} fusion(f32[448,2048]{1,0:T(8,128)S(1)} %fusion.3, bf16[448,512]{1,0:T(8,128)(2,1)S(1)} %get-tuple-element.30, bf16[1,512,2048]{2,1,0:T(8,128)(2,1)S(1)} %copy-done.1), kind=kOutput, calls=%fused_computation.5 | convolution fusion | flops 941359104 | bytes 8060928 | tf_op jit(solution)/shard_map/dot_general | solution.py:330
  74.7 27.3 %shard_map.207 = bf16[8,56,512]{2,1,0:T(8,128)(2,1)} custom-call(bf16[8,56,2048]{2,1,0:T(8,128)(2,1)} %bitcast.81), custom_call_target="tpu_custom_call" | custom-call | tf_op jit(solution)/shard_map/pallas_call | solution.py:235
  102.0 2.3 %gather_fusion.3 = bf16[256,512]{1,0:T(8,128)(2,1)S(1)} fusion(bf16[448,512]{1,0:T(8,128)(2,1)} %bitcast.80, s32[1024]{0:T(1024)S(1)} %pad_clamp_fusion), kind=kCustom, calls=%fused_computation.3 | custom fusion | bytes 525312 | tf_op jit(solution)/shard_map/gather | solution.py:346
  104.3 0.3 reshape.143
  104.6 0.4 fusion.38
  105.1 6.7 %all_gather.6 = bf16[128,2048]{1,0:T(8,128)(2,1)S(1)} all-gather(bf16[128,512]{1,0:T(8,128)(2,1)S(1)} %fusion.23), channel_id=1, replica_groups=mesh['sp'=8,'tp'=4] {'tp'}, dimensions={1}, use_global_device_ids=true | all-gather | bytes 655360 | tf_op jit(solution)/shard_map/all_gather | solution.py:350
  111.8 1.7 copy.37
  113.5 1.7 copy.38
  115.2 2.8 %convert_multiply_fusion.3 = (f32[512,128]{0,1:T(8,128)S(1)}, bf16[512,128]{0,1:T(8,128)(2,1)}, bf16[128,512]{1,0:T(8,128)(2,1)}) fusion(bf16[512,128]{0,1:T(8,128)(2,1)} %copy.37, bf16[512,128]{0,1:T(8,128)(2,1)} %copy.38, bf16[128,2048]{1,0:T(8,128)(2,1)S(1)} %all_gather.6, bf16[2048,512]{1,0:T(8,128)(2,1)} %param.29), kind=kOutput, calls=%fused_computation.35 | convolution fusion | flops 268894208 | bytes 3407872 | tf_op jit(solution)/shard_map/dot_general | solution.py:351
  118.0 1.3 collective-permute-start
  119.3 0.8 copy.58
  120.1 6.5 %all-to-all-start = ((bf16[128,8,256]{2,0,1:T(8,128)(2,1)}), bf16[128,8,256]{2,0,1:T(8,128)(2,1)S(1)}, u32[]{:S(2)}, u32[]{:S(2)}) async-start(bf16[128,8,256]{2,0,1:T(8,128)(2,1)} %bitcast.79), calls=%async_computation | async-start | bytes 1048576 | tf_op jit(solution)/shard_map/all_to_all | solution.py:354
  126.7 4.3 %fusion.1 = bf16[1,512,2048]{2,1,0:T(8,128)(2,1)} fusion(bf16[448,512]{1,0:T(8,128)(2,1)S(1)} %get-tuple-element.30, bf16[448,2048]{1,0:T(8,128)(2,1)} %bitcast.88), kind=kOutput, calls=%fused_computation.10 | convolution fusion | flops 940572672 | bytes 4390912 | tf_op jit(solution)/shard_map/dot_general | solution.py:336
  131.0 2.7 %fusion.2 = bf16[1,512,2048]{2,1,0:T(8,128)(2,1)} fusion(bf16[448,2048]{1,0:T(8,128)(2,1)S(1)} %bitcast.91, f32[448,512]{1,0:T(8,128)S(1)} %copy-done.17, f32[448,512]{1,0:T(8,128)S(1)} %copy-done.15), kind=kOutput, calls=%fused_computation.11 | convolution fusion | flops 941948928 | bytes 5767168 | tf_op jit(solution)/shard_map/dot_general | solution.py:339
  133.7 2.6 %fusion = bf16[1,512,2048]{2,1,0:T(8,128)(2,1)} fusion(bf16[448,512]{1,0:T(8,128)(2,1)S(1)} %copy-done.7, bf16[448,2048]{1,0:T(8,128)(2,1)S(1)} %bitcast.89), kind=kOutput, calls=%fused_computation.9 | convolution fusion | flops 940572672 | bytes 4390912 | tf_op jit(solution)/shard_map/dot_general | solution.py:333
  136.6 0.8 copy.41
  137.5 0.8 copy.42
  138.2 0.8 copy.43
  139.0 6.6 %all-to-all-done = bf16[128,8,256]{2,0,1:T(8,128)(2,1)S(1)} async-done(((bf16[128,8,256]{2,0,1:T(8,128)(2,1)}), bf16[128,8,256]{2,0,1:T(8,128)(2,1)S(1)}, u32[]{:S(2)}, u32[]{:S(2)}) %all-to-all-start) | async-done | bytes 524320 | tf_op jit(solution)/shard_map/all_to_all | solution.py:354
  145.6 17.3 %all-gather.2.cloned.1.call-done = bf16[1024,512]{1,0:T(8,128)(2,1)} async-done(((bf16[128,512]{1,0:T(8,128)(2,1)}), bf16[1024,512]{1,0:T(8,128)(2,1)}) %all-gather.2.cloned.1.call-update) | async-done | bytes 1048592 | tf_op jit(solution)/shard_map/all_gather | solution.py:289
  162.8 2.5 %fusion.40 = f32[256,512]{1,0:T(8,128)} fusion(bf16[1024,256]{1,0:T(8,128)(2,1)S(1)} %bitcast.83, bf16[1024,512]{1,0:T(8,128)(2,1)} %all-gather.2.cloned.1.call-done), kind=kOutput, calls=%fused_computation.89 | convolution fusion | flops 268435456 | bytes 2097152 | tf_op jit(solution)/shard_map/dot_general | solution.py:355
  (59 shorter events, 1.3 us)
Async XLA Ops:
  7.2 57.8 %copy-start = (bf16[1,512,2048]{2,1,0:T(8,128)(2,1)S(1)}, bf16[1,512,2048]{2,1,0:T(8,128)(2,1)}, u32[]{:S(2)}) copy-start(bf16[1,512,2048]{2,1,0:T(8,128)(2,1)} %param.21) | copy-start | bytes 6291460
  7.2 155.6 %all-gather.2.cloned.1.call-start = ((), (), s32[]{:S(2)}) async-start(), calls=%async_computation.1 | async-start | bytes 1179648 | tf_op jit(solution)/shard_map/all_gather | solution.py:289
  64.9 1.2 copy-start.2
  64.9 4.1 %copy-start.4 = (bf16[1,8,56,2048]{3,2,1,0:T(8,128)(2,1)}, bf16[1,8,56,2048]{3,2,1,0:T(8,128)(2,1)S(1)}, u32[]{:S(2)}) copy-start(bf16[1,8,56,2048]{3,2,1,0:T(8,128)(2,1)S(1)} %get-tuple-element.28) | copy-start | bytes 5505028
  64.9 2.9 %copy-start.1 = (bf16[1,512,2048]{2,1,0:T(8,128)(2,1)S(1)}, bf16[1,512,2048]{2,1,0:T(8,128)(2,1)}, u32[]{:S(2)}) copy-start(bf16[1,512,2048]{2,1,0:T(8,128)(2,1)} %param.22) | copy-start | bytes 6291460
  67.8 1.2 copy-start.14
  67.8 1.9 %copy-start.13 = (bf16[1,512,2048]{2,1,0:T(8,128)(2,1)S(1)}, bf16[1,512,2048]{2,1,0:T(8,128)(2,1)}, u32[]{:S(2)}) copy-start(bf16[1,512,2048]{2,1,0:T(8,128)(2,1)} %param.23) | copy-start | bytes 6291460
  69.0 2.2 %copy-start.16 = (f32[448,512]{1,0:T(8,128)}, f32[448,512]{1,0:T(8,128)S(1)}, u32[]{:S(2)}) copy-start(f32[448,512]{1,0:T(8,128)S(1)} %fusion.8) | copy-start | bytes 2752516
  71.2 1.1 copy-start.6
  105.1 12.8 %copy-start.8 = (bf16[128,512]{1,0:T(8,128)(2,1)}, bf16[128,512]{1,0:T(8,128)(2,1)S(1)}, u32[]{:S(2)}) copy-start(bf16[128,512]{1,0:T(8,128)(2,1)S(1)} %fusion.23) | copy-start | bytes 393220
  118.0 19.4 %collective-permute-start = (f32[512,2]{0,1:T(2,128)S(1)}, f32[512,2]{0,1:T(2,128)S(1)}, u32[]{:S(2)}, u32[]{:S(2)}) collective-permute-start(f32[512,2]{0,1:T(2,128)S(1)} %slice.59), channel_id=1, source_target_pairs={{4,0},{8,4},{12,8},{16,12},{20,16},{24,20},{28,24},{5,1},{9,5},{13... | collective-permute-start | bytes 12296 | tf_op jit(solution)/shard_map/ppermute | solution.py:252
  120.1 25.5 %all-to-all-start = ((bf16[128,8,256]{2,0,1:T(8,128)(2,1)}), bf16[128,8,256]{2,0,1:T(8,128)(2,1)S(1)}, u32[]{:S(2)}, u32[]{:S(2)}) async-start(bf16[128,8,256]{2,0,1:T(8,128)(2,1)} %bitcast.79), calls=%async_computation | async-start | bytes 1048576 | tf_op jit(solution)/shard_map/all_to_all | solution.py:354
  126.6 4.3 %copy-start.5 = (bf16[1,8,56,2048]{3,2,1,0:T(8,128)(2,1)S(1)}, bf16[1,8,56,2048]{3,2,1,0:T(8,128)(2,1)}, u32[]{:S(2)}) copy-start(bf16[1,8,56,2048]{3,2,1,0:T(8,128)(2,1)} %copy-done.4) | copy-start | bytes 5505028
  126.6 4.3 %copy-start.15 = (f32[448,512]{1,0:T(8,128)S(1)}, f32[448,512]{1,0:T(8,128)}, u32[]{:S(2)}) copy-start(f32[448,512]{1,0:T(8,128)} %copy-done.14) | copy-start | bytes 2752516
  126.6 4.3 %copy-start.17 = (f32[448,512]{1,0:T(8,128)S(1)}, f32[448,512]{1,0:T(8,128)}, u32[]{:S(2)}) copy-start(f32[448,512]{1,0:T(8,128)} %copy-done.16) | copy-start | bytes 2752516
  130.9 2.7 %copy-start.3 = (bf16[1,8,56,2048]{3,2,1,0:T(8,128)(2,1)S(1)}, bf16[1,8,56,2048]{3,2,1,0:T(8,128)(2,1)}, u32[]{:S(2)}) copy-start(bf16[1,8,56,2048]{3,2,1,0:T(8,128)(2,1)} %copy-done.2) | copy-start | bytes 5505028
  130.9 2.7 %copy-start.7 = (bf16[448,512]{1,0:T(8,128)(2,1)S(1)}, bf16[448,512]{1,0:T(8,128)(2,1)}, u32[]{:S(2)}) copy-start(bf16[448,512]{1,0:T(8,128)(2,1)} %copy-done.6) | copy-start | bytes 1376260
  133.6 2.7 %copy-start.12 = (f32[3,512]{1,0:T(4,128)S(1)}, f32[3,512]{1,0:T(4,128)}, u32[]{:S(2)}) copy-start(f32[3,512]{1,0:T(4,128)} %param.28) | copy-start | bytes 18436
  133.6 2.7 %copy-start.10 = (bf16[512,128]{1,0:T(8,128)(2,1)S(1)}, bf16[512,128]{1,0:T(8,128)(2,1)}, u32[]{:S(2)}) copy-start(bf16[512,128]{1,0:T(8,128)(2,1)} %param.25) | copy-start | bytes 393220
  133.6 2.8 %copy-start.11 = (bf16[512,128]{1,0:T(8,128)(2,1)S(1)}, bf16[512,128]{1,0:T(8,128)(2,1)}, u32[]{:S(2)}) copy-start(bf16[512,128]{1,0:T(8,128)(2,1)} %param.26) | copy-start | bytes 393220
  133.7 2.9 %copy-start.9 = (bf16[512,128]{0,1:T(8,128)(2,1)S(1)}, bf16[512,128]{0,1:T(8,128)(2,1)}, u32[]{:S(2)}) copy-start(bf16[512,128]{0,1:T(8,128)(2,1)} %get-tuple-element.35) | copy-start | bytes 393220
Sparse Core Ops, SparseCore 0:
  118.1 44.6 all-gather.1

commit v2 on v1

--- a/solution.py
+++ b/solution.py
@@ -134,7 +134,9 @@
     experts,
     rows,
     x_ref,
+    mixer_ref,
     out_ref,
+    mixer_all,
     from_partner,
     row_out,
     row_in,
@@ -145,8 +147,14 @@
     yr_sem,
     s_sem,
     r_sem,
+    ms_sem,
+    mr_sem,
+    ns_sem,
+    nr_sem,
 ):
     me, y, core = places(experts, rows)
+    halves = experts // 2
+    half, side_of = me // 2, lax.rem(me, 2)
     width = out_ref.shape[-1]
 
     def columns(row, side):
@@ -180,6 +188,27 @@
             send_sem=s_sem.at[step],
             recv_sem=r_sem.at[step],
             device_id={"sp": lax.rem(me + step, experts)},
+            device_id_type=MESH,
+        )
+
+    def mixer_along(hop):
+        return pltpu.make_async_remote_copy(
+            src_ref=mixer_ref,
+            dst_ref=mixer_all.at[me],
+            send_sem=ms_sem.at[hop],
+            recv_sem=mr_sem.at[hop],
+            device_id={"sp": lax.rem(half + hop, halves) * 2 + side_of},
+            device_id_type=MESH,
+        )
+
+    def mixer_beside(hop, own):
+        source = lax.rem(half - hop + halves, halves) * 2 + side_of
+        return pltpu.make_async_remote_copy(
+            src_ref=mixer_ref if own else mixer_all.at[source],
+            dst_ref=mixer_all.at[source],
+            send_sem=ns_sem.at[hop],
+            recv_sem=nr_sem.at[hop],
+            device_id={"sp": half * 2 + 1 - side_of},
             device_id_type=MESH,
         )
 
@@ -209,6 +238,10 @@
     greet(experts, rows)
     for hop in [*range(1, rows), 0]:
         to_partner(hop).start()
+    for hop in range(1, halves):
+        mixer_along(hop).start()
+    mixer_beside(0, True).start()
+    mixer_all[me] = mixer_ref[...]
     for hop in range(1, rows):
         to_partner(hop).wait_recv()
         loop(1, functools.partial(send_row, hop))
@@ -216,6 +249,9 @@
     to_partner(0).wait_recv()
     loop(1, send_across)
     out_ref[me] = whole(0)
+    for hop in range(1, halves):
+        mixer_along(hop).wait_recv()
+        mixer_beside(hop, False).start()
 
     def finish(step):
         for hop in range(1, rows):
@@ -225,25 +261,33 @@
     loop(1, lambda step: across(step).wait())
     for hop in range(rows):
         to_partner(hop).wait_send()
-
-
-def combine(partial, experts, rows):
+    for hop in range(halves):
+        mixer_beside(hop, False).wait()
+    for hop in range(1, halves):
+        mixer_along(hop).wait_send()
+
+
+def combine(partial, mixer, experts, rows):
     _, slots, full = partial.shape
     width = full // (2 * rows)
     dma = pltpu.SemaphoreType.DMA
     held = pltpu.VMEM((rows, experts, slots, width), partial.dtype)
     return pl.pallas_call(
         functools.partial(combine_kernel, experts, rows),
-        out_shape=jax.ShapeDtypeStruct((experts, slots, width), partial.dtype),
-        in_specs=[pl.BlockSpec(memory_space=pltpu.VMEM)],
-        out_specs=pl.BlockSpec(memory_space=pltpu.VMEM),
+        out_shape=(
+            jax.ShapeDtypeStruct((experts, slots, width), partial.dtype),
+            jax.ShapeDtypeStruct((experts, *mixer.shape), mixer.dtype),
+        ),
+        in_specs=[pl.BlockSpec(memory_space=pltpu.VMEM)] * 2,
+        out_specs=(pl.BlockSpec(memory_space=pltpu.VMEM),) * 2,
         scratch_shapes=[held] * 3
         + [pltpu.VMEM((experts, slots, width), partial.dtype)]
         + [dma((rows,))] * 2
         + [dma((rows, experts))] * 2
-        + [dma((experts,))] * 2,
+        + [dma((experts,))] * 2
+        + [dma((experts // 2,))] * 4,
         compiler_params=pltpu.CompilerParams(collective_id=1, has_side_effects=True),
-    )(partial)
+    )(partial, mixer)
 
 
 def from_behind(value, axis, steps):
@@ -286,7 +330,6 @@
     capacity = -(-capacity // 8) * 8
     tp_rows = lax.axis_size("tp") // 2
     mixer_out = (outer_gate.astype(jnp.float32) * conv_out.astype(jnp.float32)).astype(jnp.bfloat16)
-    mixer_all = lax.all_gather(mixer_out.T, "sp", axis=0, tiled=True)
     entry_count = 2 * tok_rows
     expert_ids = (INNER * group_choice[:, None] + inner_pair).reshape(-1)
     onehot = (expert_ids[:, None] == jnp.arange(experts, dtype=jnp.int32)[None, :]).astype(
@@ -339,9 +382,13 @@
     grad_w_down = lax.dot_general(
         hidden, scaled_rows, row_dims, preferred_element_type=jnp.float32
     ).astype(jnp.bfloat16)
-    returned = combine(
-        partial_rows.astype(jnp.bfloat16).reshape(experts, capacity, model_width), experts, tp_rows
-    )
+    returned, mixer_all = combine(
+        partial_rows.astype(jnp.bfloat16).reshape(experts, capacity, model_width),
+        mixer_out.T,
+        experts,
+        tp_rows,
+    )
+    mixer_all = mixer_all.reshape(-1, mixer_all.shape[-1])
     back_tok = (
         returned.reshape(-1, col_piece)[target].reshape(tok_rows, 2, col_piece).astype(jnp.float32)
     )

time: 173 us -> 151 us (0.87)
  waiting for transfers between devices: 23.8 us -> 1.87 us
  between operations: 14.5 us -> 1.04 us
  Pallas kernels: 65.6 us -> 75.3 us
  matrix products: 22 us -> 24.8 us
    all_gather x1 -> x0, waiting for transfers between devices: 17.3 us -> none  [per_device(): mixer_all = lax.all_gather(mixer_out.T, 'sp', axis=0, tiled=True)]
    pallas_call x1, Pallas kernels: 27.3 us -> 37 us  [combine(): pl.pallas_call(functools.partial(combine_kernel, experts, rows), out_shap...]
    all_to_all x1, waiting for transfers between devices: 6.56 us -> 1.87 us  [per_device(): lax.all_to_all(grad_rows, 'sp', split_axis=1, concat_axis=0, tiled=True)]
    dot_general x1, matrix products: 2.36 us -> 5.03 us  [per_device(): jnp.dot(grad_up, up_weight, preferred_element_type=jnp.float32)]
    dot_general x1, matrix products: 2.79 us -> 0.46 us  [per_device(): lax.dot_general(w_out, grad_rows, (((0,), (1,)), ((), ())), preferred_ele...]
    dot_general x1, matrix products: 2.68 us -> 4.86 us  [per_device(): lax.dot_general(hidden, scaled_rows, row_dims, preferred_element_type=jnp...]
    dot_general x1, matrix products: 1.12 us -> 2.93 us  [per_device(): jnp.dot(grad_gate, gate_weight, preferred_element_type=jnp.float32)]
    unnamed x43 -> x45, local copies, waits for them, and re-layouts: 8.37 us -> 7.32 us
  transfers between devices with their start and end apart: 3 -> 2, of which waited for: 2 -> 1; matrix products, arithmetic and copies ran while one was open for 8% -> 9% of each run, Pallas kernels for 0% -> 0%
where the time goes in v2:
time: 151 us; the launch traced here: 150 us
  Pallas kernels  75.3 us (50%)
  local copies, waits for them, and re-layouts  26.6 us (18%)
  matrix products  24.8 us (16%)
  starting transfers between devices  7.17 us (5%)
  blocking collectives  6.57 us (4%)
  other arithmetic  6.54 us (4%)
  waiting for transfers between devices  1.87 us (1%)
    pallas_call x1, Pallas kernels, dispatch(): pl.pallas_call(functools.partial(dispatch_kernel, experts, rows), out_sha...  38.3 us
    pallas_call x1, Pallas kernels, combine(): pl.pallas_call(functools.partial(combine_kernel, experts, rows), out_shap...  37 us
    unnamed x45, local copies, waits for them, and re-layouts  7.32 us
    all_gather x1, blocking collectives, per_device(): grad_rows = lax.all_gather(own_cols, 'tp', axis=1, tiled=True)  6.57 us
    all_to_all x1, starting transfers between devices, per_device(): lax.all_to_all(grad_rows, 'sp', split_axis=1, concat_axis=0, tiled=True)  5.89 us
    dot_general x1, matrix products, per_device(): jnp.dot(grad_up, up_weight, preferred_element_type=jnp.float32)  5.03 us
    dot_general x1, matrix products, per_device(): lax.dot_general(hidden, scaled_rows, row_dims, preferred_element_type=jnp...  4.86 us
    gather x1, local copies, waits for them, and re-layouts, pack_rows(): routing_flat[entry_of][:, None] * cot_rows[token_of].astype(jnp.float32)  3.16 us
  transfers between devices with their start and end apart: 2, of which 1 were waited for; matrix products, arithmetic and copies ran while one was open for 9% of the time, Pallas kernels for 0%

profile of v2, /device:TPU:0, one launch (start us, length us, event | category | flops | bytes accessed | tf_op | source)
XLA Modules:
  0.0 149.9 jit_solution(12448063629753710663)
XLA Ops:
  0.6 0.8 broadcast_multiply_fusion.1
  1.5 0.7 broadcast_multiply_fusion
  2.3 0.1 eq.29
  2.4 0.1 eq.25
  2.5 0.6 reduce-window.6
  3.1 0.2 slice_reduce_fusion
  3.5 0.1 mul.125
  3.8 1.4 scatter_custom_fusion
  5.2 0.7 reduce_max.9
  5.9 0.7 fusion.35
  6.6 0.7 divide_multiply_fusion
  7.4 0.1 reshape.140
  7.6 3.2 %gather_fusion.1 = f32[448]{0:T(512)S(1)} fusion(f32[256]{0:T(256)S(1)} %reshape.140, s32[1024]{0:T(1024)S(1)} %get-tuple-element.47), kind=kCustom, calls=%fused_computation.1 | custom fusion | bytes 5376 | tf_op jit(solution)/shard_map/gather | solution.py:301
  10.9 1.0 constant_dynamic-slice_fusion
  11.9 2.1 %gather_fusion.2 = bf16[448,512]{1,0:T(8,128)(2,1)S(1)} fusion(bf16[128,512]{1,0:T(8,128)(2,1)S(1)} %get-tuple-element.46, s32[1024]{0:T(1024)S(1)} %get-tuple-element.48), kind=kCustom, calls=%fused_computation.2 | custom fusion | bytes 919296 | tf_op jit(solution)/shard_map/gather | solution.py:301
  14.0 2.1 %gather_fusion = bf16[448,512]{1,0:T(8,128)(2,1)S(1)} fusion(bf16[128,512]{1,0:T(8,128)(2,1)S(1)} %get-tuple-element.45, s32[1024]{0:T(1024)S(1)} %get-tuple-element.48), kind=kCustom, calls=%fused_computation | custom fusion | bytes 919296 | tf_op jit(solution)/shard_map/gather | solution.py:300
  16.3 0.2 fusion.13
  16.5 1.0 pad_maximum_fusion.x_ref
  17.5 38.3 %shard_map.206 = bf16[2,8,56,2048]{3,2,1,0:T(8,128)(2,1)} custom-call(bf16[2,8,56,512]{3,2,1,0:T(8,128)(2,1)} %pad_maximum_fusion.x_ref), custom_call_target="tpu_custom_call" | custom-call | tf_op jit(solution)/shard_map/pallas_call | solution.py:123
  55.8 2.5 %fusion.38 = (bf16[1,8,56,2048]{3,2,1,0:T(8,128)(2,1)S(1)}, bf16[1,8,56,2048]{3,2,1,0:T(8,128)(2,1)S(1)}) fusion(bf16[2,8,56,2048]{3,2,1,0:T(8,128)(2,1)} %shard_map.206), kind=kLoop, calls=%fused_computation.87 | loop fusion | bytes 7340032 | tf_op jit(solution)/shard_map/slice | solution.py:357
  58.4 1.1 fusion.5
  59.6 1.7 %copy-done.2 = bf16[1,512,2048]{2,1,0:T(8,128)(2,1)S(1)} copy-done((bf16[1,512,2048]{2,1,0:T(8,128)(2,1)S(1)}, bf16[1,512,2048]{2,1,0:T(8,128)(2,1)}, u32[]{:S(2)}) %copy-start.2) | copy-done | bytes 2097176
  61.3 1.2 fusion.8
  62.6 0.7 copy-done.16
  63.2 1.4 multiply_convert_fusion.1
  64.7 0.8 copy-done.8
  65.4 2.9 %fusion.3 = f32[448,2048]{1,0:T(8,128)} fusion(bf16[448,512]{1,0:T(8,128)(2,1)S(1)} %get-tuple-element.35, bf16[1,512,2048]{2,1,0:T(8,128)(2,1)S(1)} %copy-done), kind=kOutput, calls=%fused_computation.12 | convolution fusion | flops 939524096 | bytes 6225920 | tf_op jit(solution)/shard_map/dot_general | solution.py:373
  68.6 5.0 %add_convert_fusion = bf16[448,2048]{1,0:T(8,128)(2,1)} fusion(f32[448,2048]{1,0:T(8,128)} %fusion.3, bf16[448,512]{1,0:T(8,128)(2,1)S(1)} %get-tuple-element.34, bf16[1,512,2048]{2,1,0:T(8,128)(2,1)} %param.22), kind=kOutput, calls=%fused_computation.5 | convolution fusion | flops 941359104 | bytes 8060928 | tf_op jit(solution)/shard_map/dot_general | solution.py:373
  73.6 0.7 fusion.27.mixer_ref
  74.3 37.0 %shard_map.207 = (bf16[8,56,512]{2,1,0:T(8,128)(2,1)}, bf16[8,128,512]{2,1,0:T(8,128)(2,1)}) custom-call(bf16[8,56,2048]{2,1,0:T(8,128)(2,1)} %bitcast.76, bf16[128,512]{1,0:T(8,128)(2,1)} %fusion.27.mixer_ref), custom_call_target="tpu_custom_call" | custom-call | tf_op jit(solution)/shard_map/pallas_call | solution.py:275
  111.3 3.0 %gather_fusion.3 = bf16[256,512]{1,0:T(8,128)(2,1)} fusion(bf16[448,512]{1,0:T(8,128)(2,1)} %bitcast.77, s32[1024]{0:T(1024)S(1)} %pad_clamp_fusion), kind=kCustom, calls=%fused_computation.3 | custom fusion | bytes 525312 | tf_op jit(solution)/shard_map/gather | solution.py:393
  114.3 1.3 reshape.144
  115.6 0.4 fusion.39
  116.1 0.6 copy-done.10
  116.8 6.6 %all_gather.3 = bf16[128,2048]{1,0:T(8,128)(2,1)S(1)} all-gather(bf16[128,512]{1,0:T(8,128)(2,1)S(1)} %fusion.24), channel_id=1, replica_groups=mesh['sp'=8,'tp'=4] {'tp'}, dimensions={1}, use_global_device_ids=true | all-gather | bytes 655360 | tf_op jit(solution)/shard_map/all_gather | solution.py:397
  123.4 0.5 convert_multiply_fusion.3
  123.8 0.7 copy-done.6
  124.5 1.3 collective-permute-start
  125.8 1.0 copy.39
  126.8 5.9 %all-to-all-start = ((bf16[128,8,256]{0,2,1:T(8,128)(2,1)}), bf16[128,8,256]{0,2,1:T(8,128)(2,1)S(1)}, u32[]{:S(2)}, u32[]{:S(2)}) async-start(bf16[128,8,256]{0,2,1:T(8,128)(2,1)} %bitcast.19), calls=%async_computation | async-start | bytes 1048576 | tf_op jit(solution)/shard_map/all_to_all | solution.py:401
  132.7 4.9 %fusion.2 = bf16[1,512,2048]{2,1,0:T(8,128)(2,1)} fusion(bf16[448,2048]{1,0:T(8,128)(2,1)} %bitcast.85, f32[448,512]{1,0:T(8,128)} %copy-done.18, f32[448,512]{1,0:T(8,128)} %copy-done.17), kind=kOutput, calls=%fused_computation.11 | convolution fusion | flops 941948928 | bytes 5767168 | tf_op jit(solution)/shard_map/dot_general | solution.py:382
  137.6 2.6 %fusion.1 = bf16[1,512,2048]{2,1,0:T(8,128)(2,1)} fusion(bf16[448,512]{1,0:T(8,128)(2,1)S(1)} %get-tuple-element.34, bf16[448,2048]{1,0:T(8,128)(2,1)S(1)} %bitcast.82), kind=kOutput, calls=%fused_computation.10 | convolution fusion | flops 940572672 | bytes 4390912 | tf_op jit(solution)/shard_map/dot_general | solution.py:379
  140.2 2.6 %fusion = bf16[1,512,2048]{2,1,0:T(8,128)(2,1)} fusion(bf16[448,512]{1,0:T(8,128)(2,1)S(1)} %copy-done.9, bf16[448,2048]{1,0:T(8,128)(2,1)S(1)} %bitcast.83), kind=kOutput, calls=%fused_computation.9 | convolution fusion | flops 940572672 | bytes 4390912 | tf_op jit(solution)/shard_map/dot_general | solution.py:376
  143.1 0.8 copy.42
  144.0 0.8 copy.43
  144.8 0.8 copy.44
  145.6 1.9 %all-to-all-done = bf16[128,8,256]{0,2,1:T(8,128)(2,1)S(1)} async-done(((bf16[128,8,256]{0,2,1:T(8,128)(2,1)}), bf16[128,8,256]{0,2,1:T(8,128)(2,1)S(1)}, u32[]{:S(2)}, u32[]{:S(2)}) %all-to-all-start) | async-done | bytes 524320 | tf_op jit(solution)/shard_map/all_to_all | solution.py:401
  147.4 2.5 %convolution_bitcast_fusion = f32[256,512]{1,0:T(8,128)} fusion(bf16[8,128,512]{2,1,0:T(8,128)(2,1)} %get-tuple-element.11, bf16[128,8,256]{0,2,1:T(8,128)(2,1)S(1)} %all-to-all-done), kind=kOutput, calls=%fused_computation.21 | convolution fusion | flops 268435456 | bytes 2097152 | tf_op jit(solution)/shard_map/dot_general | solution.py:402
  (59 shorter events, 1.6 us)
Async XLA Ops:
  0.6 57.7 %copy-start = (bf16[1,512,2048]{2,1,0:T(8,128)(2,1)S(1)}, bf16[1,512,2048]{2,1,0:T(8,128)(2,1)}, u32[]{:S(2)}) copy-start(bf16[1,512,2048]{2,1,0:T(8,128)(2,1)} %param.21) | copy-start | bytes 6291460
  58.3 1.2 copy-start.3
  58.3 4.2 %copy-start.5 = (bf16[1,8,56,2048]{3,2,1,0:T(8,128)(2,1)}, bf16[1,8,56,2048]{3,2,1,0:T(8,128)(2,1)S(1)}, u32[]{:S(2)}) copy-start(bf16[1,8,56,2048]{3,2,1,0:T(8,128)(2,1)S(1)} %get-tuple-element.32) | copy-start | bytes 5505028
  58.4 2.9 %copy-start.2 = (bf16[1,512,2048]{2,1,0:T(8,128)(2,1)S(1)}, bf16[1,512,2048]{2,1,0:T(8,128)(2,1)}, u32[]{:S(2)}) copy-start(bf16[1,512,2048]{2,1,0:T(8,128)(2,1)} %param.22) | copy-start | bytes 6291460
  61.3 1.3 copy-start.17
  61.3 1.9 %copy-start.16 = (bf16[1,512,2048]{2,1,0:T(8,128)(2,1)S(1)}, bf16[1,512,2048]{2,1,0:T(8,128)(2,1)}, u32[]{:S(2)}) copy-start(bf16[1,512,2048]{2,1,0:T(8,128)(2,1)} %param.23) | copy-start | bytes 6291460
  62.5 2.1 %copy-start.18 = (f32[448,512]{1,0:T(8,128)}, f32[448,512]{1,0:T(8,128)S(1)}, u32[]{:S(2)}) copy-start(f32[448,512]{1,0:T(8,128)S(1)} %fusion.8) | copy-start | bytes 2752516
  64.6 0.8 copy-start.8
  65.4 2.9 %copy-start.11 = (bf16[512,128]{1,0:T(8,128)(2,1)S(1)}, bf16[512,128]{1,0:T(8,128)(2,1)}, u32[]{:S(2)}) copy-start(bf16[512,128]{1,0:T(8,128)(2,1)} %param.24) | copy-start | bytes 393220
  65.4 3.1 %copy-start.12 = (bf16[512,128]{1,0:T(8,128)(2,1)S(1)}, bf16[512,128]{1,0:T(8,128)(2,1)}, u32[]{:S(2)}) copy-start(bf16[512,128]{1,0:T(8,128)(2,1)} %param.27) | copy-start | bytes 393220
  115.6 7.7 %copy-start.1 = (bf16[2048,512]{1,0:T(8,128)(2,1)S(1)}, bf16[2048,512]{1,0:T(8,128)(2,1)}, u32[]{:S(2)}) copy-start(bf16[2048,512]{1,0:T(8,128)(2,1)} %param.29) | copy-start | bytes 6291460
  116.1 0.7 copy-start.10
  123.8 0.7 copy-start.6
  124.5 19.4 %collective-permute-start = (f32[512,2]{0,1:T(2,128)S(1)}, f32[512,2]{0,1:T(2,128)S(1)}, u32[]{:S(2)}, u32[]{:S(2)}) collective-permute-start(f32[512,2]{0,1:T(2,128)S(1)} %slice.59), channel_id=1, source_target_pairs={{4,0},{8,4},{12,8},{16,12},{20,16},{24,20},{28,24},{5,1},{9,5},{13... | collective-permute-start | bytes 12296 | tf_op jit(solution)/shard_map/ppermute | solution.py:296
  126.8 20.6 %all-to-all-start = ((bf16[128,8,256]{0,2,1:T(8,128)(2,1)}), bf16[128,8,256]{0,2,1:T(8,128)(2,1)S(1)}, u32[]{:S(2)}, u32[]{:S(2)}) async-start(bf16[128,8,256]{0,2,1:T(8,128)(2,1)} %bitcast.19), calls=%async_computation | async-start | bytes 1048576 | tf_op jit(solution)/shard_map/all_to_all | solution.py:401
  132.7 4.9 %copy-start.4 = (bf16[1,8,56,2048]{3,2,1,0:T(8,128)(2,1)S(1)}, bf16[1,8,56,2048]{3,2,1,0:T(8,128)(2,1)}, u32[]{:S(2)}) copy-start(bf16[1,8,56,2048]{3,2,1,0:T(8,128)(2,1)} %copy-done.3) | copy-start | bytes 5505028
  137.6 2.6 %copy-start.9 = (bf16[448,512]{1,0:T(8,128)(2,1)S(1)}, bf16[448,512]{1,0:T(8,128)(2,1)}, u32[]{:S(2)}) copy-start(bf16[448,512]{1,0:T(8,128)(2,1)} %copy-done.8) | copy-start | bytes 1376260
  140.2 2.7 %copy-start.15 = (f32[3,512]{1,0:T(4,128)S(1)}, f32[3,512]{1,0:T(4,128)}, u32[]{:S(2)}) copy-start(f32[3,512]{1,0:T(4,128)} %param.28) | copy-start | bytes 18436
  140.2 2.7 %copy-start.13 = (bf16[512,128]{1,0:T(8,128)(2,1)S(1)}, bf16[512,128]{1,0:T(8,128)(2,1)}, u32[]{:S(2)}) copy-start(bf16[512,128]{1,0:T(8,128)(2,1)} %param.25) | copy-start | bytes 393220
  140.2 2.8 %copy-start.14 = (bf16[512,128]{1,0:T(8,128)(2,1)S(1)}, bf16[512,128]{1,0:T(8,128)(2,1)}, u32[]{:S(2)}) copy-start(bf16[512,128]{1,0:T(8,128)(2,1)} %param.26) | copy-start | bytes 393220
  140.2 3.7 %copy-start.7 = (f32[512,128]{0,1:T(8,128)S(1)}, f32[512,128]{0,1:T(8,128)}, u32[]{:S(2)}) copy-start(f32[512,128]{0,1:T(8,128)} %copy-done.6) | copy-start | bytes 786436
